TPU v7x, 32 devices: a whole 2x2x4 slice. The times are simulated.
32 devices in a mesh: ep: 16 (over z, y, core), tp: 2 (over x).
Axes of the slice: x: 2, y: 2, z: 4, core: 2. Of those that a mesh axis runs over, the one named last changes fastest.
Arguments:
- resid: bfloat16 [256, 2048], P('ep'), may hold values from -40 to 40
- queries: bfloat16 [256, 1024], P('ep', 'tp'), may hold values from -146 to 146
- new_keys: bfloat16 [256, 512], P('ep', 'tp'), may hold values from -6 to 6
- new_values: bfloat16 [256, 512], P('ep', 'tp'), may hold values from -18 to 18
- key_cache: bfloat16 [256, 4, 256, 128], P('ep', 'tp'), may hold values from -5 to 5
- value_cache: bfloat16 [256, 4, 256, 128], P('ep', 'tp'), may hold values from -18 to 18
- cum_gate: float32 [256, 8, 256], P('ep', 'tp'), may hold values from -256 to 0, as said below
- forget_logit: float32 [256, 8], P('ep', 'tp'), may hold values from -6 to 6
- forget_bias: float32 [8], P('tp'), may hold values from -3 to 2
- lengths: int32 [256], P('ep'), may hold values from 32 to 256
- out_weight: bfloat16 [1024, 2048], P('tp'), may hold values from -0.1875 to 0.1875
- norm_gain: float32 [2048], replicated, may hold values from 0.1 to 1.9
- mix_vector: bfloat16 [2048], replicated, may hold values from -0.125 to 0.125
- routes: int32 [256, 2], P('ep'), may hold values from 0 to 3, all different within a row; in each aligned block of 16 rows (0 to 15, 16 to 31, ...) at most 16 rows name the same one
- route_weight: float32 [256, 2], P('ep'), may hold values from 0.2 to 1
- expert_gate: bfloat16 [16, 2048, 768], P('ep', 'tp'), may hold values from -0.125 to 0.125
- expert_up: bfloat16 [16, 2048, 768], P('ep', 'tp'), may hold values from -0.125 to 0.125
- expert_down: bfloat16 [16, 768, 2048], P('ep', None, 'tp'), may hold values from -0.109375 to 0.109375
- dense_gate: bfloat16 [2048, 3072], P('tp', 'ep'), may hold values from -0.125 to 0.125
- dense_up: bfloat16 [2048, 3072], P('tp', 'ep'), may hold values from -0.125 to 0.125
- dense_down: bfloat16 [3072, 2048], P('ep', 'tp'), may hold values from -0.109375 to 0.109375
Outputs:
- layer_out: bfloat16 [256, 2048], P('ep', 'tp')
Inputs may be any that keep to these rules, and one draw needn't show every extreme that they name: `routes`: each row names 2 different experts; the rows of one index of ep name no expert more than 16 times. `cum_gate`: for positions below the sequence's length, the running sum of the log forget gates of positions 0 to p; it never rises along p.
All inputs are finite; a program needn't handle non-finite values.
Results may differ from a plain program's by a relative error of at most 0.0095.
Values may be sent and summed in bfloat16 or wider, within the bound.
No kernel may reach another device: no remote copies, remote signals or barrier semaphores. Data moves between devices by JAX's collectives and lax.ppermute only.
A program may use at most 64 MiB of HBM per device.

v0:
```python
import math

import jax
import jax.numpy as jnp
from jax import lax
from jax.sharding import PartitionSpec as P

QUERY_HEADS = 8
KV_HEADS = 4
HEAD = 128
TOP_K = 2
EXP_SPAN = 4


EPSILON = 1e-06


def slot_table(route_block, expert_ids, capacity):
    blocks = route_block.shape[0]
    flat_routes = route_block.reshape(blocks, 1, -1)
    matched = (flat_routes == expert_ids.reshape(1, -1, 1)).astype(jnp.int32)
    ranking = jnp.cumsum(matched, axis=2) - 1
    slot_ids = jnp.arange(capacity, dtype=jnp.int32)
    taken = (matched[..., None] > 0) & (ranking[..., None] == slot_ids)
    table = jnp.swapaxes(taken, 2, 3).astype(jnp.float32)
    return table.reshape(
        blocks, expert_ids.shape[0], capacity, route_block.shape[1], route_block.shape[2]
    )


def attend(
    queries,
    new_keys,
    new_values,
    key_cache,
    value_cache,
    cum_gate,
    forget_logit,
    forget_bias,
    lengths,
):
    seqcount = queries.shape[0]
    kv_local = key_cache.shape[1]
    grouping = QUERY_HEADS // KV_HEADS
    heads_local = kv_local * grouping
    scale_factor = 1.0 / math.sqrt(HEAD)
    query_float = queries.astype(jnp.float32).reshape(seqcount, kv_local, grouping, HEAD)
    scores = jnp.einsum("sgjd,sgpd->sgjp", query_float, key_cache.astype(jnp.float32))
    scores = scores.reshape(seqcount, heads_local, -1) * scale_factor
    own_score = jnp.einsum(
        "sgjd,sgd->sgj", query_float, new_keys.astype(jnp.float32).reshape(seqcount, kv_local, HEAD)
    )
    own_score = own_score.reshape(seqcount, heads_local) * scale_factor
    log_forget = jax.nn.log_sigmoid(forget_logit + forget_bias)
    position = jnp.arange(cum_gate.shape[2], dtype=jnp.int32)
    latest = jnp.sum(jnp.where(position == (lengths - 1)[:, None, None], cum_gate, 0.0), axis=2)
    scores = scores + (latest + log_forget)[:, :, None] - cum_gate
    visible = position[None, None, :] < lengths[:, None, None]
    scores = jnp.where(visible, scores, -jnp.inf)
    highest = jnp.maximum(jnp.max(scores, axis=2), own_score)
    weights_past = jnp.exp(scores - highest[:, :, None])
    weight_own = jnp.exp(own_score - highest)
    totals = jnp.sum(weights_past, axis=2) + weight_own
    probs_past = (weights_past / totals[:, :, None]).astype(jnp.bfloat16)
    prob_own = (weight_own / totals).astype(jnp.bfloat16)
    mixed = jnp.einsum(
        "sgjp,sgpd->sgjd",
        probs_past.astype(jnp.float32).reshape(seqcount, kv_local, grouping, -1),
        value_cache.astype(jnp.float32),
    )
    mixed = mixed + prob_own.astype(jnp.float32).reshape(
        seqcount, kv_local, grouping, 1
    ) * new_values.astype(jnp.float32).reshape(seqcount, kv_local, 1, HEAD)
    return mixed.reshape(seqcount, heads_local * HEAD).astype(jnp.bfloat16)


def body(
    resid,
    queries,
    new_keys,
    new_values,
    key_cache,
    value_cache,
    cum_gate,
    forget_logit,
    forget_bias,
    lengths,
    out_weight,
    norm_gain,
    mix_vector,
    routes,
    route_weight,
    expert_gate,
    expert_up,
    expert_down,
    dense_gate,
    dense_up,
    dense_down,
):
    attended = attend(
        queries,
        new_keys,
        new_values,
        key_cache,
        value_cache,
        cum_gate,
        forget_logit,
        forget_bias,
        lengths,
    )
    head_part = jnp.dot(attended, out_weight, preferred_element_type=jnp.float32)
    projected = lax.psum(head_part.astype(jnp.bfloat16), "tp")
    state_full = resid.astype(jnp.float32) + projected.astype(jnp.float32)
    inverse = lax.rsqrt(jnp.mean(state_full * state_full, axis=1) + EPSILON)
    scaled_full = state_full * norm_gain
    gate = jax.nn.sigmoid(inverse * jnp.sum(scaled_full * mix_vector.astype(jnp.float32), axis=1))
    channel_width = resid.shape[1] // lax.axis_size("tp")
    offset = lax.axis_index("tp") * channel_width
    state = lax.dynamic_slice_in_dim(state_full, offset, channel_width, 1)
    normed = (
        lax.dynamic_slice_in_dim(scaled_full, offset, channel_width, 1) * inverse[:, None]
    ).astype(jnp.bfloat16)
    ep_count = lax.axis_size("ep")
    tokens = resid.shape[0]
    experts = ep_count // EXP_SPAN
    capacity = min(tokens, 2 * ((tokens * TOP_K + experts - 1) // experts))
    w_gate = expert_gate[0]
    w_up = expert_up[0]
    w_down = expert_down[0]
    table = slot_table(
        routes.reshape(1, tokens, TOP_K), jnp.arange(experts, dtype=jnp.int32), capacity
    )[0]
    picked = jnp.sum(table, axis=3).astype(jnp.bfloat16)
    outgoing = jnp.einsum("ect,td->ecd", picked, normed, preferred_element_type=jnp.float32).astype(
        jnp.bfloat16
    )
    outgoing = jnp.repeat(outgoing, EXP_SPAN, axis=0)
    arrived = lax.all_to_all(outgoing, "ep", split_axis=0, concat_axis=0, tiled=True)
    flat_rows = arrived.reshape(-1, arrived.shape[2])
    gated = lax.psum(
        jnp.dot(flat_rows, w_gate, preferred_element_type=jnp.float32).astype(jnp.bfloat16), "tp"
    ).astype(jnp.float32)
    upped = lax.psum(
        jnp.dot(flat_rows, w_up, preferred_element_type=jnp.float32).astype(jnp.bfloat16), "tp"
    ).astype(jnp.float32)
    hidden = (jax.nn.silu(gated) * upped).astype(jnp.bfloat16)
    produced = jnp.dot(hidden, w_down, preferred_element_type=jnp.float32)
    produced = produced.reshape(arrived.shape[0], arrived.shape[1], -1)
    returned = lax.all_to_all(
        produced.astype(jnp.bfloat16), "ep", split_axis=0, concat_axis=0, tiled=True
    ).astype(produced.dtype)
    outputs = returned.reshape(experts, EXP_SPAN, capacity, -1).sum(axis=1)
    routed = jnp.einsum(
        "ectk,tk,ecd->td", table, route_weight, outputs, precision=lax.Precision.HIGHEST
    )
    piece = lax.all_gather(normed, "ep", axis=0, tiled=True)
    paired = jnp.concatenate(
        [
            jnp.dot(piece, dense_gate, preferred_element_type=jnp.float32),
            jnp.dot(piece, dense_up, preferred_element_type=jnp.float32),
        ],
        axis=1,
    )
    paired = lax.psum(paired.astype(jnp.bfloat16), "tp").astype(jnp.float32)
    hidden_width = dense_gate.shape[1]
    dense_hidden = (jax.nn.silu(paired[:, :hidden_width]) * paired[:, hidden_width:]).astype(
        jnp.bfloat16
    )
    dense = lax.psum_scatter(
        jnp.dot(dense_hidden, dense_down, preferred_element_type=jnp.float32),
        "ep",
        scatter_dimension=0,
        tiled=True,
    )
    result = state + routed + gate[:, None] * dense
    return result.astype(jnp.bfloat16)


def solution(mesh):
    placed = (
        P("ep", None),
        P("ep", "tp"),
        P("ep", "tp"),
        P("ep", "tp"),
        P("ep", "tp", None, None),
        P("ep", "tp", None, None),
        P("ep", "tp", None),
        P("ep", "tp"),
        P("tp"),
        P("ep"),
        P("tp", None),
        P(),
        P(),
        P("ep", None),
        P("ep", None),
        P("ep", "tp", None),
        P("ep", "tp", None),
        P("ep", None, "tp"),
        P("tp", "ep"),
        P("tp", "ep"),
        P("ep", "tp"),
    )
    return jax.shard_map(body, mesh=mesh, in_specs=placed, out_specs=P("ep", "tp"), check_vma=False)
```

profile of v0, /device:TPU:0, one launch (start us, length us, event | category | flops | bytes accessed | tf_op | source)
XLA Modules:
  0.0 187.2 jit_solution(820209216632114887)
XLA Ops:
  6.6 0.8 broadcast_add_fusion.1
  7.4 0.7 iota_compare_fusion.2
  8.1 0.7 reshape.220
  8.9 2.2 %convolution_multiply_fusion = f32[16,2,2,256]{3,2,1,0:T(2,128)S(1)} fusion(bf16[16,2,2,128]{3,2,1,0:T(2,128)(2,1)S(1)} %reshape.220, bf16[16,2,256,128]{3,2,1,0:T(8,128)(2,1)} %param.25), kind=kOutput, calls=%fused_computation.14 | convolution fusion | flops 4210688 | bytes 2179072 | tf_op jit(solution)/shard_map/sgjd,sgpd->sgjp/dot_general | solution.py:48
  12.7 2.0 %fusion.18 = bf16[16,2,2,128]{3,2,1,0:T(2,128)(2,1)S(1)} fusion(bf16[16,2,2,256]{3,2,1,0:T(2,128)(2,1)S(1)} %reshape.222, bf16[16,2,256,128]{3,2,1,0:T(8,128)(2,1)} %param.26, f32[16,2,128]{2,1,0:T(2,128)S(1)} %reshape.227, f32[16,2,2]{2,1,0:T(2,128)S(1)} %copy.39), kind=kOutput, calls=%fused_computation.19 | convolution fusion | flops 4218880 | bytes 2162944 | tf_op jit(solution)/shard_map/sgjp,sgpd->sgjd/dot_general | solution.py:66
  14.8 1.0 convolution_convert_fusion
  16.6 23.0 %all-reduce.4.cloned.1.call-done = bf16[16,2048]{1,0:T(8,128)(2,1)} async-done(((bf16[16,2048]{1,0:T(8,128)(2,1)}), bf16[16,2048]{1,0:T(8,128)(2,1)}) %all-reduce.4.cloned.1.call-update) | async-done | bytes 65552 | tf_op jit(solution)/shard_map/psum | solution.py:112
  39.7 1.0 multiply_reduce_fusion
  40.7 0.5 add_divide_fusion.1
  41.3 0.6 copy-done.6
  42.1 0.9 broadcast_in_dim.42
  43.0 5.6 %all-to-all-start = ((bf16[16,16,1024]{2,1,0:T(8,128)(2,1)}), bf16[16,16,1024]{2,1,0:T(8,128)(2,1)S(1)}, u32[]{:S(2)}, u32[]{:S(2)}) async-start(bf16[16,16,1024]{2,1,0:T(8,128)(2,1)} %bitcast.10), calls=%async_computation | async-start | bytes 1048576 | tf_op jit(solution)/shard_map/all_to_all | solution.py:138
  48.6 26.9 %all_gather.3 = bf16[256,1024]{1,0:T(8,128)(2,1)S(1)} all-gather(bf16[16,1024]{1,0:T(8,128)(2,1)} %copy-done.6), channel_id=1, replica_groups=mesh['ep'=16,'tp'=2] {'ep'}, dimensions={0}, use_global_device_ids=true | all-gather | bytes 557056 | tf_op jit(solution)/shard_map/all_gather | solution.py:156
  76.2 0.7 pad_maximum_fusion
  76.9 2.9 %fusion.12 = bf16[256,768]{1,0:T(8,128)(2,1)} fusion(bf16[256,1024]{1,0:T(8,128)(2,1)S(1)} %bitcast.66, bf16[1,1024,768]{2,1,0:T(8,128)(2,1)} %param.37), kind=kOutput, calls=%fused_computation.9 | convolution fusion | flops 402849792 | bytes 2490368 | tf_op jit(solution)/shard_map/dot_general | solution.py:144
  79.8 1.3 fusion.9
  81.1 36.3 %all-reduce.6.cloned.1.call-done = (bf16[256,768]{1,0:T(8,128)(2,1)}, bf16[256,768]{1,0:T(8,128)(2,1)}, bf16[256,384]{0,1:T(8,128)(2,1)}) async-done(((bf16[256,768]{1,0:T(8,128)(2,1)}, bf16[256,768]{1,0:T(8,128)(2,1)}, bf16[256,384]{0,1:T(8,128)(2,1)}), (bf16[256,768]{1,0:T(8,128)(2,1)}, bf16[256,768]{1,0:T(8,128)(2,1)}, bf16[256,384]{0,1:T(8,128)(2,1)})) %all-reduce.6.cloned.1.call-update) | async-done | bytes 983056 | tf_op jit(solution)/shard_map/psum | solution.py:143
  117.4 1.0 convert_element_type.111
  118.5 1.4 fusion.27
  120.2 2.8 %fusion.6 = bf16[16,16,1024]{2,1,0:T(8,128)(2,1)} fusion(bf16[16,16,768]{2,1,0:T(8,128)(2,1)S(1)} %bitcast.65, bf16[1,768,1024]{2,1,0:T(8,128)(2,1)} %param.38), kind=kOutput, calls=%fused_computation.7 | convolution fusion | flops 402915328 | bytes 2490368 | tf_op jit(solution)/shard_map/dot_general | solution.py:147
  123.0 5.6 %all-to-all-start.1 = ((bf16[16,16,1024]{2,1,0:T(8,128)(2,1)}), bf16[16,16,1024]{2,1,0:T(8,128)(2,1)S(1)}, u32[]{:S(2)}, u32[]{:S(2)}) async-start(bf16[16,16,1024]{2,1,0:T(8,128)(2,1)} %fusion.6), calls=%async_computation.1 | async-start | bytes 1048576 | tf_op jit(solution)/shard_map/all_to_all | solution.py:149
  128.9 13.9 %all-to-all-done.1 = bf16[16,16,1024]{2,1,0:T(8,128)(2,1)S(1)} async-done(((bf16[16,16,1024]{2,1,0:T(8,128)(2,1)}), bf16[16,16,1024]{2,1,0:T(8,128)(2,1)S(1)}, u32[]{:S(2)}, u32[]{:S(2)}) %all-to-all-start.1) | async-done | bytes 524320 | tf_op jit(solution)/shard_map/all_to_all | solution.py:149
  143.0 35.8 %reduce-scatter.2.cloned.1.call-done = f32[16,1024]{1,0:T(8,128)} async-done(((f32[256,1024]{1,0:T(8,128)}), f32[16,1024]{1,0:T(8,128)}) %reduce-scatter.2.cloned.1.call-update) | async-done | bytes 65552 | tf_op jit(solution)/shard_map/reduce_scatter | solution.py:169
  178.8 1.9 %fusion.17 = bf16[16,1024]{1,0:T(8,128)(2,1)} fusion(f32[4,16,1024]{2,1,0:T(8,128)S(1)} %convert_reduce_fusion, f32[16,1024]{1,0:T(8,128)} %reduce-scatter.2.cloned.1.call-done, f32[16,2048]{1,0:T(8,128)S(1)} %get-tuple-element.12, s32[]{:T(128)S(6)} %select_n.19, f32[16,1,4,16]{3,1,2,0:T(1,128)S(1)} %fusion.25, f32[16]{0:T(128)S(1)} %copy-done.13), kind=kOutput, calls=%fused_computation.17 | convolution fusion | flops 12648448 | bytes 430148 | tf_op jit(solution)/shard_map/ectk,tk,ecd->td/dot_general | solution.py:153
  (84 shorter events, 4.1 us)
Async XLA Ops:
  6.5 8.2 %copy-start = (bf16[512,2048]{1,0:T(8,128)(2,1)S(1)}, bf16[512,2048]{1,0:T(8,128)(2,1)}, u32[]{:S(2)}) copy-start(bf16[512,2048]{1,0:T(8,128)(2,1)} %param.31) | copy-start | bytes 6291460
  6.5 4.7 %copy-start.14 = (f32[16,4]{0,1:T(4,128)S(1)}, f32[16,4]{0,1:T(4,128)}, u32[]{:S(2)}) copy-start(f32[16,4]{0,1:T(4,128)} %param.28) | copy-start | bytes 772
  6.5 4.8 %copy-start.9 = (bf16[16,256]{1,0:T(8,128)(2,1)S(1)}, bf16[16,256]{1,0:T(8,128)(2,1)}, u32[]{:S(2)}) copy-start(bf16[16,256]{1,0:T(8,128)(2,1)} %param.23) | copy-start | bytes 24580
  6.5 5.1 %copy-start.7 = (f32[16,4,256]{2,1,0:T(4,128)S(1)}, f32[16,4,256]{2,1,0:T(4,128)}, u32[]{:S(2)}) copy-start(f32[16,4,256]{2,1,0:T(4,128)} %param.27) | copy-start | bytes 196612
  6.5 5.3 %copy-start.17 = (f32[4]{0:T(128)S(1)}, f32[4]{0:T(128)}, u32[]{:S(2)}) copy-start(f32[4]{0:T(128)} %param.29) | copy-start | bytes 52
  6.5 6.0 %copy-start.10 = (bf16[16,256]{1,0:T(8,128)(2,1)S(1)}, bf16[16,256]{1,0:T(8,128)(2,1)}, u32[]{:S(2)}) copy-start(bf16[16,256]{1,0:T(8,128)(2,1)} %param.24) | copy-start | bytes 24580
  6.6 33.1 %all-reduce.4.cloned.1.call-start = ((), (), s32[]{:S(2)}) async-start(), calls=%async_computation.3 | async-start | bytes 131072 | tf_op jit(solution)/shard_map/psum | solution.py:112
  12.7 3.1 %copy-start.12 = (bf16[2048]{0:T(1024)(128)(2,1)S(1)}, bf16[2048]{0:T(1024)(128)(2,1)}, u32[]{:S(2)}) copy-start(bf16[2048]{0:T(1024)(128)(2,1)} %param.33) | copy-start | bytes 12292
  12.7 3.2 %copy-start.15 = (s32[16,2]{0,1:T(2,128)S(1)}, s32[16,2]{0,1:T(2,128)}, u32[]{:S(2)}) copy-start(s32[16,2]{0,1:T(2,128)} %param.34) | copy-start | bytes 388
  12.7 27.0 %copy-start.8 = (bf16[16,2048]{1,0:T(8,128)(2,1)S(1)}, bf16[16,2048]{1,0:T(8,128)(2,1)}, u32[]{:S(2)}) copy-start(bf16[16,2048]{1,0:T(8,128)(2,1)} %param.21) | copy-start | bytes 196612
  12.7 27.0 %copy-start.11 = (f32[2048]{0:T(1024)S(1)}, f32[2048]{0:T(1024)}, u32[]{:S(2)}) copy-start(f32[2048]{0:T(1024)} %param.32) | copy-start | bytes 24580
  15.8 59.7 %copy-start.1 = (bf16[1024,192]{0,1:T(8,128)(2,1)S(1)}, bf16[1024,192]{0,1:T(8,128)(2,1)}, u32[]{:S(2)}) copy-start(bf16[1024,192]{0,1:T(8,128)(2,1)} %param.40) | copy-start | bytes 1179652
  15.8 60.1 %copy-start.2 = (bf16[1024,192]{0,1:T(8,128)(2,1)S(1)}, bf16[1024,192]{0,1:T(8,128)(2,1)}, u32[]{:S(2)}) copy-start(bf16[1024,192]{0,1:T(8,128)(2,1)} %param.39) | copy-start | bytes 1179652
  41.3 0.6 copy-start.6
  43.0 33.9 %all-to-all-start = ((bf16[16,16,1024]{2,1,0:T(8,128)(2,1)}), bf16[16,16,1024]{2,1,0:T(8,128)(2,1)S(1)}, u32[]{:S(2)}, u32[]{:S(2)}) async-start(bf16[16,16,1024]{2,1,0:T(8,128)(2,1)} %bitcast.10), calls=%async_computation | async-start | bytes 1048576 | tf_op jit(solution)/shard_map/all_to_all | solution.py:138
  48.6 68.8 %all-reduce.6.cloned.1.call-start = ((), (), s32[]{:S(2)}) async-start(), calls=%async_computation.5 | async-start | bytes 1966080 | tf_op jit(solution)/shard_map/psum | solution.py:143
  76.9 2.9 %copy-start.18 = (bf16[1,1024,768]{2,1,0:T(8,128)(2,1)S(1)}, bf16[1,1024,768]{2,1,0:T(8,128)(2,1)}, u32[]{:S(2)}) copy-start(bf16[1,1024,768]{2,1,0:T(8,128)(2,1)} %param.36) | copy-start | bytes 4718596
  79.8 38.7 %copy-start.3 = (bf16[192,1024]{1,0:T(8,128)(2,1)S(1)}, bf16[192,1024]{1,0:T(8,128)(2,1)}, u32[]{:S(2)}) copy-start(bf16[192,1024]{1,0:T(8,128)(2,1)} %param.41) | copy-start | bytes 1179652
  81.1 97.7 %reduce-scatter.2.cloned.1.call-start = ((), (), s32[]{:S(2)}) async-start(), calls=%async_computation.4 | async-start | bytes 1114112 | tf_op jit(solution)/shard_map/reduce_scatter | solution.py:169
  117.4 2.5 %copy-start.4 = (bf16[256,768]{1,0:T(8,128)(2,1)S(1)}, bf16[256,768]{1,0:T(8,128)(2,1)}, u32[]{:S(2)}) copy-start(bf16[256,768]{1,0:T(8,128)(2,1)} %get-tuple-element.5) | copy-start | bytes 1179652
  117.4 2.5 %copy-start.5 = (bf16[256,768]{1,0:T(8,128)(2,1)S(1)}, bf16[256,768]{1,0:T(8,128)(2,1)}, u32[]{:S(2)}) copy-start(bf16[256,768]{1,0:T(8,128)(2,1)} %get-tuple-element.6) | copy-start | bytes 1179652
  119.9 8.7 %copy-start.16 = (f32[16,2]{0,1:T(2,128)S(1)}, f32[16,2]{0,1:T(2,128)}, u32[]{:S(2)}) copy-start(f32[16,2]{0,1:T(2,128)} %param.35) | copy-start | bytes 388
  120.2 58.6 %copy-start.13 = (f32[16]{0:T(128)S(1)}, f32[16]{0:T(128)}, u32[]{:S(2)}) copy-start(f32[16]{0:T(128)} %get-tuple-element.14) | copy-start | bytes 196
  123.0 19.9 %all-to-all-start.1 = ((bf16[16,16,1024]{2,1,0:T(8,128)(2,1)}), bf16[16,16,1024]{2,1,0:T(8,128)(2,1)S(1)}, u32[]{:S(2)}, u32[]{:S(2)}) async-start(bf16[16,16,1024]{2,1,0:T(8,128)(2,1)} %fusion.6), calls=%async_computation.1 | async-start | bytes 1048576 | tf_op jit(solution)/shard_map/all_to_all | solution.py:149
Sparse Core Ops, SparseCore 0:
  15.9 23.6 all-reduce.3
  81.2 36.1 all-reduce.5
  121.1 57.6 reduce-scatter.1
where the time goes:
time: 188 us; the launch traced here: 187 us
  waiting for transfers between devices  109 us (58%)
  blocking collectives  26.9 us (14%)
  matrix products  16.8 us (9%)
  between operations  13.4 us (7%)
  starting transfers between devices  11.4 us (6%)
  other arithmetic  6.26 us (3%)
  local copies, waits for them, and re-layouts  3.38 us (2%)
    psum x1, waiting for transfers between devices, body(): lax.psum(jnp.dot(flat_rows, w_up, preferred_element_type=jnp.float32).ast...  36.3 us
    reduce_scatter x1, waiting for transfers between devices, body(): lax.psum_scatter(jnp.dot(dense_hidden, dense_down, preferred_element_type...  35.8 us
    all_gather x1, blocking collectives, body(): piece = lax.all_gather(normed, 'ep', axis=0, tiled=True)  26.9 us
    psum x1, waiting for transfers between devices, body(): projected = lax.psum(head_part.astype(jnp.bfloat16), 'tp')  23 us
    all_to_all x1, waiting for transfers between devices, body(): lax.all_to_all(produced.astype(jnp.bfloat16), 'ep', split_axis=0, concat_...  13.9 us
    all_to_all x1, starting transfers between devices, body(): lax.all_to_all(outgoing, 'ep', split_axis=0, concat_axis=0, tiled=True)  5.62 us
    all_to_all x1, starting transfers between devices, body(): lax.all_to_all(produced.astype(jnp.bfloat16), 'ep', split_axis=0, concat_...  5.62 us
  transfers between devices with their start and end apart: 5, of which 4 were waited for; matrix products, arithmetic and copies ran while one was open for 3% of the time, Pallas kernels for 0%

commit v1 on v0

--- a/solution.py
+++ b/solution.py
@@ -74,7 +74,7 @@
     return mixed.reshape(seqcount, heads_local * HEAD).astype(jnp.bfloat16)
 
 
-def body(
+def slot_body(
     resid,
     queries,
     new_keys,
@@ -176,6 +176,155 @@
     return result.astype(jnp.bfloat16)
 
 
+def exchange(rows, axis, distance):
+    count = lax.axis_size(axis)
+    return lax.ppermute(rows, axis, [(i, i ^ distance) for i in range(count)])
+
+
+def rows_body(
+    resid,
+    queries,
+    new_keys,
+    new_values,
+    key_cache,
+    value_cache,
+    cum_gate,
+    forget_logit,
+    forget_bias,
+    lengths,
+    out_weight,
+    norm_gain,
+    mix_vector,
+    routes,
+    route_weight,
+    expert_gate,
+    expert_up,
+    expert_down,
+    dense_gate,
+    dense_up,
+    dense_down,
+):
+    ep_count = lax.axis_size("ep")
+    tokens, width = resid.shape
+    experts = ep_count // EXP_SPAN
+    channel_width = width // 2
+    side = lax.axis_index("tp")
+    attended = attend(
+        queries,
+        new_keys,
+        new_values,
+        key_cache,
+        value_cache,
+        cum_gate,
+        forget_logit,
+        forget_bias,
+        lengths,
+    )
+    head_part = jnp.dot(attended, out_weight, preferred_element_type=jnp.float32)
+    head_part = head_part.astype(jnp.bfloat16)
+    other_part = exchange(head_part, "tp", 1)
+    projected = head_part.astype(jnp.float32) + other_part.astype(jnp.float32)
+    projected = projected.astype(jnp.bfloat16)
+    state_full = resid.astype(jnp.float32) + projected.astype(jnp.float32)
+    inverse = lax.rsqrt(jnp.mean(state_full * state_full, axis=1) + EPSILON)
+    scaled_full = state_full * norm_gain
+    gate = jax.nn.sigmoid(inverse * jnp.sum(scaled_full * mix_vector.astype(jnp.float32), axis=1))
+    offset = side * channel_width
+    state = lax.dynamic_slice_in_dim(state_full, offset, channel_width, 1)
+    normed = (
+        lax.dynamic_slice_in_dim(scaled_full, offset, channel_width, 1) * inverse[:, None]
+    ).astype(jnp.bfloat16)
+    chosen = routes[:, :, None] == jnp.arange(experts, dtype=jnp.int32)
+    shares = jnp.sum(jnp.where(chosen, route_weight[:, :, None], 0.0), axis=1)
+    shares = jnp.concatenate([gate[:, None], shares], axis=1)
+    high = shares.astype(jnp.bfloat16)
+    low = (shares - high.astype(jnp.float32)).astype(jnp.bfloat16)
+    filler = (-2 * shares.shape[1]) % 128
+    payload = jnp.concatenate(
+        [normed, high, low, jnp.zeros((tokens, filler), jnp.bfloat16)], axis=1
+    )
+    own_expert = lax.axis_index("ep") // EXP_SPAN
+    columns = 1 + experts
+
+    w_gate, w_up, w_down = expert_gate[0], expert_up[0], expert_down[0]
+
+    def partials(rows):
+        x = rows[:, :channel_width]
+        parts = [
+            jnp.dot(x, w, preferred_element_type=jnp.float32)
+            for w in (w_gate, w_up, dense_gate, dense_up)
+        ]
+        joined = jnp.concatenate(parts, axis=1)
+        half = rows.shape[0] // 2
+        mine = lax.dynamic_slice_in_dim(joined, side * half, half, 0)
+        theirs = lax.dynamic_slice_in_dim(joined, (1 - side) * half, half, 0)
+        extra = rows[:, channel_width:].astype(jnp.float32)
+        weights = extra[:, :columns] + extra[:, columns : 2 * columns]
+        weights = lax.dynamic_slice_in_dim(weights, side * half, half, 0)
+        return mine, theirs.astype(jnp.bfloat16), weights
+
+    span = w_gate.shape[1]
+    dense_span = dense_gate.shape[1]
+
+    def hidden_rows(mine, arrived, weights):
+        total = mine + arrived.astype(jnp.float32)
+        gated, upped = total[:, :span], total[:, span : 2 * span]
+        d_gated = total[:, 2 * span : 2 * span + dense_span]
+        d_upped = total[:, 2 * span + dense_span :]
+        share = lax.dynamic_slice_in_dim(weights, 1 + own_expert, 1, 1)
+        hidden = jax.nn.silu(gated) * upped * share
+        d_hidden = jax.nn.silu(d_gated) * d_upped * weights[:, :1]
+        return jnp.concatenate([hidden, d_hidden], axis=1).astype(jnp.bfloat16)
+
+    def downward(mine, arrived):
+        first = jnp.where(side == 0, mine, arrived)
+        second = jnp.where(side == 0, arrived, mine)
+        hidden = jnp.concatenate([first, second], axis=0)
+        out = jnp.dot(hidden[:, :span], w_down, preferred_element_type=jnp.float32)
+        return out + jnp.dot(hidden[:, span:], dense_down, preferred_element_type=jnp.float32)
+
+    pair = jnp.concatenate([payload, exchange(payload, "ep", 2)], axis=0)
+    near = jnp.concatenate([pair, exchange(pair, "ep", 1)], axis=0)
+    groups = ep_count // 4
+    far_pairs = jnp.concatenate([exchange(pair, "ep", 4 * k) for k in range(1, groups)], axis=0)
+    far = jnp.concatenate([far_pairs, exchange(far_pairs, "ep", 1)], axis=0)
+
+    mine_n, theirs_n, weights_n = partials(near)
+    sums_n = exchange(theirs_n, "tp", 1)
+    mine_f, theirs_f, weights_f = partials(far)
+    sums_f = exchange(theirs_f, "tp", 1)
+    hidden_n = hidden_rows(mine_n, sums_n, weights_n)
+    rows_n = exchange(hidden_n, "tp", 1)
+    hidden_f = hidden_rows(mine_f, sums_f, weights_f)
+    rows_f = exchange(hidden_f, "tp", 1)
+    out_n = downward(hidden_n, rows_n)
+    out_f = downward(hidden_f, rows_f)
+
+    def fold(kept, sent, distance):
+        return kept + exchange(sent.astype(jnp.bfloat16), "ep", distance).astype(jnp.float32)
+
+    half_n = out_n.shape[0] // 2
+    own_n = fold(out_n[:half_n], out_n[half_n:], 1)
+    half_f = out_f.shape[0] // 2
+    own_f = fold(out_f[:half_f], out_f[half_f:], 1).reshape(groups - 1, 2, tokens, -1)
+    total = fold(own_n[:tokens], own_n[tokens:], 2)
+    chip_f = fold(own_f[:, 0], own_f[:, 1], 2)
+    for k in range(1, groups):
+        total = fold(total, chip_f[k - 1], 4 * k)
+    return (state + total).astype(jnp.bfloat16)
+
+
+def body(*arrays):
+    ep_count = lax.axis_size("ep")
+    tokens = arrays[0].shape[0]
+    experts = ep_count // EXP_SPAN
+    capacity = min(tokens, 2 * ((tokens * TOP_K + experts - 1) // experts))
+    powers = ep_count >= 8 and ep_count & (ep_count - 1) == 0
+    if capacity == tokens and powers and lax.axis_size("tp") == 2:
+        return rows_body(*arrays)
+    return slot_body(*arrays)
+
+
 def solution(mesh):
     placed = (
         P("ep", None),

time: 188 us -> 85.5 us (0.45)
  waiting for transfers between devices: 109 us -> 27 us
  blocking collectives: 26.9 us -> 0 us
  between operations: 13.4 us -> 0.46 us
  starting transfers between devices: 11.4 us -> 22 us
  local copies, waits for them, and re-layouts: 3.38 us -> 10.9 us
  other arithmetic: 6.26 us -> 9.35 us
    psum x2 -> x0, waiting for transfers between devices: 59.3 us -> none  [the longest x1 36.3 us: body(): lax.psum(jnp.dot(flat_rows, w_up, preferred_element_type=jnp.float32).ast...]
    reduce_scatter x1 -> x0, waiting for transfers between devices: 35.8 us -> none  [body(): lax.psum_scatter(jnp.dot(dense_hidden, dense_down, preferred_element_type...]
    ppermute x0 -> x18, waiting for transfers between devices: none -> 27 us  [exchange(): return lax.ppermute(rows, axis, [(i, i ^ distance) for i in range(count)])]
    all_gather x1 -> x0, blocking collectives: 26.9 us -> none  [body(): piece = lax.all_gather(normed, 'ep', axis=0, tiled=True)]
    ppermute x0 -> x18, starting transfers between devices: none -> 22 us  [exchange(): return lax.ppermute(rows, axis, [(i, i ^ distance) for i in range(count)])]
    all_to_all x2 -> x0, waiting for transfers between devices: 13.9 us -> none  [the longest x1 13.9 us: body(): lax.all_to_all(produced.astype(jnp.bfloat16), 'ep', split_axis=0, concat_...]
    all_to_all x2 -> x0, starting transfers between devices: 11.2 us -> none  [the longest x1 5.62 us: body(): lax.all_to_all(outgoing, 'ep', split_axis=0, concat_axis=0, tiled=True)]
    concatenate x0 -> x4, local copies, waits for them, and re-layouts: none -> 3.49 us  [the longest x2 3.37 us: partials(): joined = jnp.concatenate(parts, axis=1)]
  transfers between devices with their start and end apart: 5 -> 18, of which waited for: 4 -> 10; matrix products, arithmetic and copies ran while one was open for 3% -> 17% of each run, Pallas kernels for 0% -> 0%
where the time goes in v1:
time: 85.5 us; the launch traced here: 84.7 us
  waiting for transfers between devices  27 us (32%)
  starting transfers between devices  22 us (26%)
  matrix products  15.1 us (18%)
  local copies, waits for them, and re-layouts  10.9 us (13%)
  other arithmetic  9.35 us (11%)
    ppermute x18, waiting for transfers between devices, exchange(): return lax.ppermute(rows, axis, [(i, i ^ distance) for i in range(count)])  27 us
    ppermute x18, starting transfers between devices, exchange(): return lax.ppermute(rows, axis, [(i, i ^ distance) for i in range(count)])  22 us
    dot_general x8, matrix products, partials(): jnp.dot(x, w, preferred_element_type=jnp.float32)  9.05 us
    unnamed x48, local copies, waits for them, and re-layouts  3.59 us
    concatenate x2, local copies, waits for them, and re-layouts, partials(): joined = jnp.concatenate(parts, axis=1)  3.37 us
    dot_general x1, matrix products, attend(): jnp.einsum('sgjd,sgpd->sgjp', query_float, key_cache.astype(jnp.float32))  2.24 us
    add x2, other arithmetic, hidden_rows(): total = mine + arrived.astype(jnp.float32)  2.15 us
    dot_general x1, matrix products, attend(): jnp.einsum('sgjp,sgpd->sgjd', probs_past.astype(jnp.float32).reshape(seqc...  1.97 us
  transfers between devices with their start and end apart: 18, of which 10 were waited for; matrix products, arithmetic and copies ran while one was open for 17% of the time, Pallas kernels for 0%

profile of v1, /device:TPU:0, one launch (start us, length us, event | category | flops | bytes accessed | tf_op | source)
XLA Modules:
  0.0 84.7 jit_solution(3243249145132020390)
XLA Ops:
  4.2 2.2 %convolution_multiply_fusion = f32[16,2,2,256]{3,2,1,0:T(2,128)S(1)} fusion(bf16[16,2,2,128]{3,2,1,0:T(2,128)(2,1)S(1)} %reshape.147, bf16[16,2,256,128]{3,2,1,0:T(8,128)(2,1)} %param.25), kind=kOutput, calls=%fused_computation.15 | convolution fusion | flops 4210688 | bytes 2179072 | tf_op jit(solution)/shard_map/sgjd,sgpd->sgjp/dot_general | solution.py:48
  7.5 2.0 %fusion.18 = bf16[16,2,2,128]{3,2,1,0:T(2,128)(2,1)S(1)} fusion(bf16[16,2,2,256]{3,2,1,0:T(2,128)(2,1)S(1)} %reshape.149, bf16[16,2,256,128]{3,2,1,0:T(8,128)(2,1)} %param.26, f32[16,2,128]{2,1,0:T(2,128)S(1)} %reshape.151, f32[16,2,2]{2,1,0:T(2,128)S(1)} %copy.54), kind=kOutput, calls=%fused_computation.17 | convolution fusion | flops 4218880 | bytes 2162944 | tf_op jit(solution)/shard_map/sgjp,sgpd->sgjd/dot_general | solution.py:66
  9.9 3.0 %collective-permute-start = (bf16[16,2048]{1,0:T(8,128)(2,1)S(1)}, bf16[16,2048]{1,0:T(8,128)(2,1)S(1)}, u32[]{:S(2)}, u32[]{:S(2)}) collective-permute-start(bf16[16,2048]{1,0:T(8,128)(2,1)S(1)} %convolution_convert_fusion), channel_id=1, source_target_pairs={{0,1},{1,0},{2,3},{3,2},{4,5},{5,4},{6,7},{7,6},{8,9},{9,8},{10,11... | collective-permute-start | bytes 196616 | tf_op jit(solution)/shard_map/ppermute | solution.py:181
  13.0 2.1 %collective-permute-done = bf16[16,2048]{1,0:T(8,128)(2,1)S(1)} collective-permute-done((bf16[16,2048]{1,0:T(8,128)(2,1)S(1)}, bf16[16,2048]{1,0:T(8,128)(2,1)S(1)}, u32[]{:S(2)}, u32[]{:S(2)}) %collective-permute-start) | collective-permute-done | bytes 65568 | tf_op jit(solution)/shard_map/ppermute | solution.py:181
  15.9 2.1 %collective-permute-start.1 = (bf16[16,1152]{1,0:T(8,128)(2,1)S(1)}, bf16[16,1152]{1,0:T(8,128)(2,1)S(1)}, u32[]{:S(2)}, u32[]{:S(2)}) collective-permute-start(bf16[16,1152]{1,0:T(8,128)(2,1)S(1)} %concatenate.41), channel_id=1, source_target_pairs={{0,4},{2,6},{4,0},{6,2},{8,12},{10,14},{12,8},{14,10},{16,20},{18,... | collective-permute-start | bytes 110600 | tf_op jit(solution)/shard_map/ppermute | solution.py:181
  17.9 1.9 %collective-permute-done.1 = bf16[16,1152]{1,0:T(8,128)(2,1)S(1)} collective-permute-done((bf16[16,1152]{1,0:T(8,128)(2,1)S(1)}, bf16[16,1152]{1,0:T(8,128)(2,1)S(1)}, u32[]{:S(2)}, u32[]{:S(2)}) %collective-permute-start.1) | collective-permute-done | bytes 36896 | tf_op jit(solution)/shard_map/ppermute | solution.py:181
  20.5 4.1 %collective-permute-start.9 = (bf16[32,1152]{1,0:T(8,128)(2,1)}, bf16[32,1152]{1,0:T(8,128)(2,1)}, u32[]{:S(2)}, u32[]{:S(2)}) collective-permute-start(bf16[32,1152]{1,0:T(8,128)(2,1)} %pad_maximum_fusion.5), channel_id=1, source_target_pairs={{0,24},{2,26},{4,28},{6,30},{8,16},{10,18},{12,20},{14,22},{16,8},... | collective-permute-start | bytes 221192 | tf_op jit(solution)/shard_map/ppermute | solution.py:181
  27.0 2.5 %fusion.6 = f32[64,768]{1,0:T(8,128)} fusion(bf16[1,1024,768]{2,1,0:T(8,128)(2,1)} %param.37, bf16[64,1152]{1,0:T(8,128)(2,1)S(1)} %pad_maximum_fusion.2), kind=kOutput, calls=%fused_computation.7 | convolution fusion | flops 100663296 | bytes 1900544 | tf_op jit(solution)/shard_map/dot_general | solution.py:254
  32.6 1.7 %collective-permute-start.3 = (bf16[32,1920]{1,0:T(8,128)(2,1)S(1)}, bf16[32,1920]{1,0:T(8,128)(2,1)S(1)}, u32[]{:S(2)}, u32[]{:S(2)}) collective-permute-start(bf16[32,1920]{1,0:T(8,128)(2,1)S(1)} %dynamic-slice_convert_fusion.1), channel_id=1, source_target_pairs={{0,1},{1,0},{2,3},{3,2},{4,5},{5,4},{6,7},{7,6},{8,9},{9,8},{10,11... | collective-permute-start | bytes 368648 | tf_op jit(solution)/shard_map/ppermute | solution.py:181
  38.9 1.6 %collective-permute-start.4 = (bf16[32,960]{1,0:T(8,128)(2,1)S(1)}, bf16[32,960]{1,0:T(8,128)(2,1)S(1)}, u32[]{:S(2)}, u32[]{:S(2)}) collective-permute-start(bf16[32,960]{1,0:T(8,128)(2,1)S(1)} %pad_maximum_fusion.6), channel_id=1, source_target_pairs={{0,1},{1,0},{2,3},{3,2},{4,5},{5,4},{6,7},{7,6},{8,9},{9,8},{10,11... | collective-permute-start | bytes 184328 | tf_op jit(solution)/shard_map/ppermute | solution.py:181
  41.4 1.9 %collective-permute-done.4 = bf16[32,960]{1,0:T(8,128)(2,1)S(1)} collective-permute-done((bf16[32,960]{1,0:T(8,128)(2,1)S(1)}, bf16[32,960]{1,0:T(8,128)(2,1)S(1)}, u32[]{:S(2)}, u32[]{:S(2)}) %collective-permute-start.4) | collective-permute-done | bytes 61472 | tf_op jit(solution)/shard_map/ppermute | solution.py:181
  46.4 1.3 %fusion.8 = f32[192,768]{1,0:T(8,128)} fusion(bf16[1,1024,768]{2,1,0:T(8,128)(2,1)S(1)} %copy-done.4, bf16[192,1152]{1,0:T(8,128)(2,1)S(1)} %constant_dynamic-update-slice_fusion), kind=kOutput, calls=%fused_computation.9 | convolution fusion | flops 301989888 | bytes 2555904 | tf_op jit(solution)/shard_map/dot_general | solution.py:254
  47.8 2.2 %concatenate.49 = f32[192,1920]{1,0:T(8,128)} concatenate(f32[192,768]{1,0:T(8,128)} %fusion.8, f32[192,768]{1,0:T(8,128)S(1)} %fusion.4, f32[192,192]{1,0:T(8,128)S(1)} %copy-done.9, f32[192,192]{1,0:T(8,128)} %fusion.23), dimensions={1} | concatenate | bytes 2949120 | tf_op jit(solution)/shard_map/concatenate | solution.py:257
  50.0 1.2 %dynamic-slice_convert_fusion = bf16[96,1920]{1,0:T(8,128)(2,1)S(1)} fusion(f32[192,1920]{1,0:T(8,128)} %concatenate.49, s32[]{:T(128)S(6)} %select_n.89), kind=kLoop, calls=%fused_computation.19 | loop fusion | bytes 737284 | tf_op jit(solution)/shard_map/convert_element_type | solution.py:264
  51.1 1.6 %collective-permute-start.11 = (bf16[96,1920]{1,0:T(8,128)(2,1)S(1)}, bf16[96,1920]{1,0:T(8,128)(2,1)S(1)}, u32[]{:S(2)}, u32[]{:S(2)}) collective-permute-start(bf16[96,1920]{1,0:T(8,128)(2,1)S(1)} %dynamic-slice_convert_fusion), channel_id=1, source_target_pairs={{0,1},{1,0},{2,3},{3,2},{4,5},{5,4},{6,7},{7,6},{8,9},{9,8},{10,11... | collective-permute-start | bytes 1105928 | tf_op jit(solution)/shard_map/ppermute | solution.py:181
  53.0 7.6 %collective-permute-done.11 = bf16[96,1920]{1,0:T(8,128)(2,1)S(1)} collective-permute-done((bf16[96,1920]{1,0:T(8,128)(2,1)S(1)}, bf16[96,1920]{1,0:T(8,128)(2,1)S(1)}, u32[]{:S(2)}, u32[]{:S(2)}) %collective-permute-start.11) | collective-permute-done | bytes 368672 | tf_op jit(solution)/shard_map/ppermute | solution.py:181
  60.6 1.2 %convert_add_fusion = f32[96,1920]{1,0:T(8,128)S(1)} fusion(bf16[96,1920]{1,0:T(8,128)(2,1)S(1)} %collective-permute-done.11, f32[192,1920]{1,0:T(8,128)} %concatenate.49, s32[]{:T(128)S(6)} %select_n.88), kind=kLoop, calls=%fused_computation.18 | loop fusion | flops 368640 | bytes 1843204 | tf_op jit(solution)/shard_map/add | solution.py:270
  62.7 5.1 %collective-permute-done.12 = bf16[96,960]{1,0:T(8,128)(2,1)S(1)} collective-permute-done((bf16[96,960]{1,0:T(8,128)(2,1)S(1)}, bf16[96,960]{1,0:T(8,128)(2,1)S(1)}, u32[]{:S(2)}, u32[]{:S(2)}) %collective-permute-start.12) | collective-permute-done | bytes 184352 | tf_op jit(solution)/shard_map/ppermute | solution.py:181
  70.2 1.6 %collective-permute-start.14 = (bf16[3,16,1024]{2,1,0:T(8,128)(2,1)S(1)}, bf16[3,16,1024]{2,1,0:T(8,128)(2,1)S(1)}, u32[]{:S(2)}, u32[]{:S(2)}) collective-permute-start(bf16[3,16,1024]{2,1,0:T(8,128)(2,1)S(1)} %fusion.33), channel_id=1, source_target_pairs={{0,4},{2,6},{4,0},{6,2},{8,12},{10,14},{12,8},{14,10},{16,20},{18,... | collective-permute-start | bytes 294920 | tf_op jit(solution)/shard_map/ppermute | solution.py:181
  72.4 3.1 %collective-permute-done.14 = bf16[3,16,1024]{2,1,0:T(8,128)(2,1)S(1)} collective-permute-done((bf16[3,16,1024]{2,1,0:T(8,128)(2,1)S(1)}, bf16[3,16,1024]{2,1,0:T(8,128)(2,1)S(1)}, u32[]{:S(2)}, u32[]{:S(2)}) %collective-permute-start.14) | collective-permute-done | bytes 98336 | tf_op jit(solution)/shard_map/ppermute | solution.py:181
  75.5 1.3 %collective-permute-start.15 = (bf16[16,1024]{1,0:T(8,128)(2,1)S(1)}, bf16[16,1024]{1,0:T(8,128)(2,1)S(1)}, u32[]{:S(2)}, u32[]{:S(2)}) collective-permute-start(bf16[16,1024]{1,0:T(8,128)(2,1)S(1)} %get-tuple-element.18), channel_id=1, source_target_pairs={{0,8},{2,10},{4,12},{6,14},{8,0},{10,2},{12,4},{14,6},{16,24},{18,... | collective-permute-start | bytes 98312 | tf_op jit(solution)/shard_map/ppermute | solution.py:181
  76.9 2.4 %collective-permute-start.17 = (bf16[16,1024]{1,0:T(8,128)(2,1)S(1)}, bf16[16,1024]{1,0:T(8,128)(2,1)S(1)}, u32[]{:S(2)}, u32[]{:S(2)}) collective-permute-start(bf16[16,1024]{1,0:T(8,128)(2,1)S(1)} %get-tuple-element.19), channel_id=1, source_target_pairs={{0,24},{2,26},{4,28},{6,30},{8,16},{10,18},{12,20},{14,22},{16,8},... | collective-permute-start | bytes 98312 | tf_op jit(solution)/shard_map/ppermute | solution.py:181
  79.8 2.8 %collective-permute-done.17 = bf16[16,1024]{1,0:T(8,128)(2,1)S(1)} collective-permute-done((bf16[16,1024]{1,0:T(8,128)(2,1)S(1)}, bf16[16,1024]{1,0:T(8,128)(2,1)S(1)}, u32[]{:S(2)}, u32[]{:S(2)}) %collective-permute-start.17) | collective-permute-done | bytes 32800 | tf_op jit(solution)/shard_map/ppermute | solution.py:181
  82.6 1.5 %collective-permute-done.16 = bf16[16,1024]{1,0:T(8,128)(2,1)S(1)} collective-permute-done((bf16[16,1024]{1,0:T(8,128)(2,1)S(1)}, bf16[16,1024]{1,0:T(8,128)(2,1)S(1)}, u32[]{:S(2)}, u32[]{:S(2)}) %collective-permute-start.16) | collective-permute-done | bytes 32800 | tf_op jit(solution)/shard_map/ppermute | solution.py:181
  (144 shorter events, 26.3 us)
Async XLA Ops:
  0.0 9.5 %copy-start = (bf16[512,2048]{1,0:T(8,128)(2,1)S(1)}, bf16[512,2048]{1,0:T(8,128)(2,1)}, u32[]{:S(2)}) copy-start(bf16[512,2048]{1,0:T(8,128)(2,1)} %param.31) | copy-start | bytes 6291460
  9.5 15.7 %copy-start.5 = (bf16[1024,192]{0,1:T(8,128)(2,1)S(1)}, bf16[1024,192]{0,1:T(8,128)(2,1)}, u32[]{:S(2)}) copy-start(bf16[1024,192]{0,1:T(8,128)(2,1)} %param.39) | copy-start | bytes 1179652
  9.5 16.6 %copy-start.6 = (bf16[1024,192]{0,1:T(8,128)(2,1)S(1)}, bf16[1024,192]{0,1:T(8,128)(2,1)}, u32[]{:S(2)}) copy-start(bf16[1024,192]{0,1:T(8,128)(2,1)} %param.40) | copy-start | bytes 1179652
  9.9 5.2 %collective-permute-start = (bf16[16,2048]{1,0:T(8,128)(2,1)S(1)}, bf16[16,2048]{1,0:T(8,128)(2,1)S(1)}, u32[]{:S(2)}, u32[]{:S(2)}) collective-permute-start(bf16[16,2048]{1,0:T(8,128)(2,1)S(1)} %convolution_convert_fusion), channel_id=1, source_target_pairs={{0,1},{1,0},{2,3},{3,2},{4,5},{5,4},{6,7},{7,6},{8,9},{9,8},{10,11... | collective-permute-start | bytes 196616 | tf_op jit(solution)/shard_map/ppermute | solution.py:181
  15.9 4.0 %collective-permute-start.1 = (bf16[16,1152]{1,0:T(8,128)(2,1)S(1)}, bf16[16,1152]{1,0:T(8,128)(2,1)S(1)}, u32[]{:S(2)}, u32[]{:S(2)}) collective-permute-start(bf16[16,1152]{1,0:T(8,128)(2,1)S(1)} %concatenate.41), channel_id=1, source_target_pairs={{0,4},{2,6},{4,0},{6,2},{8,12},{10,14},{12,8},{14,10},{16,20},{18,... | collective-permute-start | bytes 110600 | tf_op jit(solution)/shard_map/ppermute | solution.py:181
  19.9 9.6 %copy-start.12 = (bf16[16,1152]{1,0:T(8,128)(2,1)}, bf16[16,1152]{1,0:T(8,128)(2,1)S(1)}, u32[]{:S(2)}) copy-start(bf16[16,1152]{1,0:T(8,128)(2,1)S(1)} %collective-permute-done.1) | copy-start | bytes 110596
  20.5 4.7 %collective-permute-start.2 = (bf16[32,1152]{1,0:T(8,128)(2,1)}, bf16[32,1152]{1,0:T(8,128)(2,1)S(1)}, u32[]{:S(2)}, u32[]{:S(2)}) collective-permute-start(bf16[32,1152]{1,0:T(8,128)(2,1)} %pad_maximum_fusion.5), channel_id=1, source_target_pairs={{0,2},{2,0},{4,6},{6,4},{8,10},{10,8},{12,14},{14,12},{16,18},{18,... | collective-permute-start | bytes 221192 | tf_op jit(solution)/shard_map/ppermute | solution.py:181
  20.5 13.8 %collective-permute-start.9 = (bf16[32,1152]{1,0:T(8,128)(2,1)}, bf16[32,1152]{1,0:T(8,128)(2,1)}, u32[]{:S(2)}, u32[]{:S(2)}) collective-permute-start(bf16[32,1152]{1,0:T(8,128)(2,1)} %pad_maximum_fusion.5), channel_id=1, source_target_pairs={{0,24},{2,26},{4,28},{6,30},{8,16},{10,18},{12,20},{14,22},{16,8},... | collective-permute-start | bytes 221192 | tf_op jit(solution)/shard_map/ppermute | solution.py:181
  24.6 9.7 %collective-permute-start.8 = (bf16[32,1152]{1,0:T(8,128)(2,1)}, bf16[32,1152]{1,0:T(8,128)(2,1)}, u32[]{:S(2)}, u32[]{:S(2)}) collective-permute-start(bf16[32,1152]{1,0:T(8,128)(2,1)} %pad_maximum_fusion.5), channel_id=1, source_target_pairs={{0,16},{2,18},{4,20},{6,22},{8,24},{10,26},{12,28},{14,30},{16,0},... | collective-permute-start | bytes 221192 | tf_op jit(solution)/shard_map/ppermute | solution.py:181
  24.6 9.7 %collective-permute-start.7 = (bf16[32,1152]{1,0:T(8,128)(2,1)}, bf16[32,1152]{1,0:T(8,128)(2,1)}, u32[]{:S(2)}, u32[]{:S(2)}) collective-permute-start(bf16[32,1152]{1,0:T(8,128)(2,1)} %pad_maximum_fusion.5), channel_id=1, source_target_pairs={{0,8},{2,10},{4,12},{6,14},{8,0},{10,2},{12,4},{14,6},{16,24},{18,... | collective-permute-start | bytes 221192 | tf_op jit(solution)/shard_map/ppermute | solution.py:181
  32.6 5.2 %collective-permute-start.3 = (bf16[32,1920]{1,0:T(8,128)(2,1)S(1)}, bf16[32,1920]{1,0:T(8,128)(2,1)S(1)}, u32[]{:S(2)}, u32[]{:S(2)}) collective-permute-start(bf16[32,1920]{1,0:T(8,128)(2,1)S(1)} %dynamic-slice_convert_fusion.1), channel_id=1, source_target_pairs={{0,1},{1,0},{2,3},{3,2},{4,5},{5,4},{6,7},{7,6},{8,9},{9,8},{10,11... | collective-permute-start | bytes 368648 | tf_op jit(solution)/shard_map/ppermute | solution.py:181
  35.3 8.6 %collective-permute-start.10 = (bf16[96,1152]{1,0:T(8,128)(2,1)S(1)}, bf16[96,1152]{1,0:T(8,128)(2,1)S(1)}, u32[]{:S(2)}, u32[]{:S(2)}) collective-permute-start(bf16[96,1152]{1,0:T(8,128)(2,1)S(1)} %pad_maximum_fusion), channel_id=1, source_target_pairs={{0,2},{2,0},{4,6},{6,4},{8,10},{10,8},{12,14},{14,12},{16,18},{18,... | collective-permute-start | bytes 663560 | tf_op jit(solution)/shard_map/ppermute | solution.py:181
  38.9 4.3 %collective-permute-start.4 = (bf16[32,960]{1,0:T(8,128)(2,1)S(1)}, bf16[32,960]{1,0:T(8,128)(2,1)S(1)}, u32[]{:S(2)}, u32[]{:S(2)}) collective-permute-start(bf16[32,960]{1,0:T(8,128)(2,1)S(1)} %pad_maximum_fusion.6), channel_id=1, source_target_pairs={{0,1},{1,0},{2,3},{3,2},{4,5},{5,4},{6,7},{7,6},{8,9},{9,8},{10,11... | collective-permute-start | bytes 184328 | tf_op jit(solution)/shard_map/ppermute | solution.py:181
  51.1 9.5 %collective-permute-start.11 = (bf16[96,1920]{1,0:T(8,128)(2,1)S(1)}, bf16[96,1920]{1,0:T(8,128)(2,1)S(1)}, u32[]{:S(2)}, u32[]{:S(2)}) collective-permute-start(bf16[96,1920]{1,0:T(8,128)(2,1)S(1)} %dynamic-slice_convert_fusion), channel_id=1, source_target_pairs={{0,1},{1,0},{2,3},{3,2},{4,5},{5,4},{6,7},{7,6},{8,9},{9,8},{10,11... | collective-permute-start | bytes 1105928 | tf_op jit(solution)/shard_map/ppermute | solution.py:181
  53.0 9.5 %copy-start.7 = (bf16[192,1024]{1,0:T(8,128)(2,1)S(1)}, bf16[192,1024]{1,0:T(8,128)(2,1)}, u32[]{:S(2)}) copy-start(bf16[192,1024]{1,0:T(8,128)(2,1)} %param.41) | copy-start | bytes 1179652
  53.0 9.5 %copy-start.10 = (bf16[32,960]{1,0:T(8,128)(2,1)S(1)}, bf16[32,960]{1,0:T(8,128)(2,1)}, u32[]{:S(2)}) copy-start(bf16[32,960]{1,0:T(8,128)(2,1)} %get-tuple-element.16) | copy-start | bytes 184324
  62.1 5.7 %collective-permute-start.12 = (bf16[96,960]{1,0:T(8,128)(2,1)S(1)}, bf16[96,960]{1,0:T(8,128)(2,1)S(1)}, u32[]{:S(2)}, u32[]{:S(2)}) collective-permute-start(bf16[96,960]{1,0:T(8,128)(2,1)S(1)} %pad_maximum_fusion.1), channel_id=1, source_target_pairs={{0,1},{1,0},{2,3},{3,2},{4,5},{5,4},{6,7},{7,6},{8,9},{9,8},{10,11... | collective-permute-start | bytes 552968 | tf_op jit(solution)/shard_map/ppermute | solution.py:181
  68.7 1.5 %collective-permute-start.13 = (bf16[96,1024]{1,0:T(8,128)(2,1)S(1)}, bf16[96,1024]{1,0:T(8,128)(2,1)S(1)}, u32[]{:S(2)}, u32[]{:S(2)}) collective-permute-start(bf16[96,1024]{1,0:T(8,128)(2,1)S(1)} %slice.249), channel_id=1, source_target_pairs={{0,2},{2,0},{4,6},{6,4},{8,10},{10,8},{12,14},{14,12},{16,18},{18,... | collective-permute-start | bytes 589832 | tf_op jit(solution)/shard_map/ppermute | solution.py:181
  69.2 2.7 %collective-permute-start.5 = (bf16[32,1024]{1,0:T(8,128)(2,1)S(1)}, bf16[32,1024]{1,0:T(8,128)(2,1)S(1)}, u32[]{:S(2)}, u32[]{:S(2)}) collective-permute-start(bf16[32,1024]{1,0:T(8,128)(2,1)S(1)} %slice.250), channel_id=1, source_target_pairs={{0,2},{2,0},{4,6},{6,4},{8,10},{10,8},{12,14},{14,12},{16,18},{18,... | collective-permute-start | bytes 196616 | tf_op jit(solution)/shard_map/ppermute | solution.py:181
  70.2 5.3 %collective-permute-start.14 = (bf16[3,16,1024]{2,1,0:T(8,128)(2,1)S(1)}, bf16[3,16,1024]{2,1,0:T(8,128)(2,1)S(1)}, u32[]{:S(2)}, u32[]{:S(2)}) collective-permute-start(bf16[3,16,1024]{2,1,0:T(8,128)(2,1)S(1)} %fusion.33), channel_id=1, source_target_pairs={{0,4},{2,6},{4,0},{6,2},{8,12},{10,14},{12,8},{14,10},{16,20},{18,... | collective-permute-start | bytes 294920 | tf_op jit(solution)/shard_map/ppermute | solution.py:181
  71.9 7.9 %collective-permute-start.6 = (bf16[16,1024]{1,0:T(8,128)(2,1)S(1)}, bf16[16,1024]{1,0:T(8,128)(2,1)S(1)}, u32[]{:S(2)}, u32[]{:S(2)}) collective-permute-start(bf16[16,1024]{1,0:T(8,128)(2,1)S(1)} %slice.251), channel_id=1, source_target_pairs={{0,4},{2,6},{4,0},{6,2},{8,12},{10,14},{12,8},{14,10},{16,20},{18,... | collective-permute-start | bytes 98312 | tf_op jit(solution)/shard_map/ppermute | solution.py:181
  75.5 4.2 %collective-permute-start.15 = (bf16[16,1024]{1,0:T(8,128)(2,1)S(1)}, bf16[16,1024]{1,0:T(8,128)(2,1)S(1)}, u32[]{:S(2)}, u32[]{:S(2)}) collective-permute-start(bf16[16,1024]{1,0:T(8,128)(2,1)S(1)} %get-tuple-element.18), channel_id=1, source_target_pairs={{0,8},{2,10},{4,12},{6,14},{8,0},{10,2},{12,4},{14,6},{16,24},{18,... | collective-permute-start | bytes 98312 | tf_op jit(solution)/shard_map/ppermute | solution.py:181
  76.9 5.7 %collective-permute-start.17 = (bf16[16,1024]{1,0:T(8,128)(2,1)S(1)}, bf16[16,1024]{1,0:T(8,128)(2,1)S(1)}, u32[]{:S(2)}, u32[]{:S(2)}) collective-permute-start(bf16[16,1024]{1,0:T(8,128)(2,1)S(1)} %get-tuple-element.19), channel_id=1, source_target_pairs={{0,24},{2,26},{4,28},{6,30},{8,16},{10,18},{12,20},{14,22},{16,8},... | collective-permute-start | bytes 98312 | tf_op jit(solution)/shard_map/ppermute | solution.py:181
  79.3 4.8 %collective-permute-start.16 = (bf16[16,1024]{1,0:T(8,128)(2,1)S(1)}, bf16[16,1024]{1,0:T(8,128)(2,1)S(1)}, u32[]{:S(2)}, u32[]{:S(2)}) collective-permute-start(bf16[16,1024]{1,0:T(8,128)(2,1)S(1)} %get-tuple-element.20), channel_id=1, source_target_pairs={{0,16},{2,18},{4,20},{6,22},{8,24},{10,26},{12,28},{14,30},{16,0},... | collective-permute-start | bytes 98312 | tf_op jit(solution)/shard_map/ppermute | solution.py:181
  (16 other events, 79.4 us)
